TPU v7x, 512 devices: a whole 4x4x16 slice. The times are simulated.
512 devices in a mesh: sp: 32 (over z, core), tp: 16 (over y, x).
Axes of the slice: x: 4, y: 4, z: 16, core: 2. Of those that a mesh axis runs over, the one named last changes fastest.
Arguments:
- residual: bfloat16 [4096, 4096], P('sp', 'tp'), may hold values from -46 to 46
- query_small: bfloat16 [4096, 2048], P('sp', 'tp'), may hold values from -6 to 6
- key_narrow_group: bfloat16 [4096, 2048], P('sp', 'tp'), may hold values from -6 to 6
- query_large: bfloat16 [4096, 4096], P('sp', 'tp'), may hold values from -6 to 6
- key_large: bfloat16 [4096, 4096], P('sp', 'tp'), may hold values from -6 to 6
- values: bfloat16 [4096, 2, 2048], P('sp', None, 'tp'), may hold values from -6 to 6
- gates: bfloat16 [4096, 2, 2048], P('sp', None, 'tp'), may hold values from -6 to 6
- log_decay: float32 [4096, 2, 16], P('sp', None, 'tp'), may hold values from -0.65 to 0, as said below
- head_gain: float32 [2, 2048], P(None, 'tp'), may hold values from 0.1 to 1.9
- out_weight: bfloat16 [2, 2048, 4096], P(None, 'sp', 'tp'), may hold values from -0.09375 to 0.09375
- norm_gain: float32 [4096], P('tp'), may hold values from 0.1 to 1.9
- routes: int32 [4096, 2], P('sp'), may hold values from 0 to 31, all different within a row; in each aligned block of 128 rows (0 to 127, 128 to 255, ...) at most 16 rows name the same one
- route_weight: float32 [4096, 2], P('sp'), may hold values from 0.2 to 1
- expert_gate: bfloat16 [32, 4096, 2048], P('sp', None, 'tp'), may hold values from -0.09375 to 0.09375
- expert_up: bfloat16 [32, 4096, 2048], P('sp', None, 'tp'), may hold values from -0.09375 to 0.09375
- expert_down: bfloat16 [32, 2048, 4096], P('sp', None, 'tp'), may hold values from -0.5 to 0.5
Outputs:
- new_stream: bfloat16 [4096, 4096], P('sp', 'tp')
Inputs may be any that keep to these rules, and one draw needn't show every extreme that they name: `routes`: each row names two different experts; in each aligned block of 128 rows no expert is named more than 16 times, a bound that some block reaches. `log_decay`: negative at every position.
All inputs are finite; a program needn't handle non-finite values.
Results may differ from a plain program's by a relative error of at most 0.019.
Values may be sent and summed in bfloat16 or wider, within the bound.
A program may use at most 64 MiB of HBM per device.

v0:
```python
import functools
import jax
import jax.numpy as jnp
from jax import lax
from jax.sharding import Mesh
from jax.sharding import PartitionSpec as P

D = 4096
SP = ("sp_0", "sp_1")
TP = ("tp_0", "tp_1")
EPS = 1e-06
THETA = 10000.0


def neutral_like(array, identity):
    return jax.tree.map(
        lambda a, e: jnp.broadcast_to(jnp.asarray(e, a.dtype), a.shape), array, identity
    )


def gathered_once(array, axis):
    leaves = jax.tree.leaves(array)
    order = sorted(range(len(leaves)), key=lambda k: -leaves[k].size)
    width = (1, *leaves[order[0]].shape)[-1]
    lines = [
        jnp.pad(leaves[k].reshape(-1), (0, -leaves[k].size % width)).reshape(-1, width)
        for k in order
    ]
    both, at, found = (lax.all_gather(jnp.concatenate(lines), axis), 0, {})
    for k, line in zip(order, lines):
        piece = both[:, at : at + len(line)].reshape(len(both), -1)
        found[k] = piece[:, : leaves[k].size].reshape(-1, *leaves[k].shape)
        at += len(line)
    numbers = iter(range(len(leaves)))
    return jax.tree.map(lambda _: found[next(numbers)], array)


def entering_2(array, axes, combine, identity):
    before = start = neutral_like(array, identity)
    so_far = array
    for axis in reversed(axes):
        devices, place = (lax.axis_size(axis), lax.axis_index(axis))
        pieces = gathered_once(so_far, axis)
        inside, so_far = (start, start)
        for k in range(devices):
            passed = k < place
            so_far = combine(so_far, jax.tree.map(lambda part: part[k], pieces))
            inside = jax.tree.map(lambda new, old: jnp.where(passed, new, old), so_far, inside)
        before = combine(inside, before)
    return before


def in_order(blocks, dim):
    lengths = list(blocks.shape[1:])
    lengths[dim] *= blocks.shape[0]
    return jnp.moveaxis(blocks, 0, dim).reshape(lengths)


def from_everyone(array, axis):
    devices = lax.axis_size(axis)
    return lax.all_to_all(
        jnp.broadcast_to(array[None], (devices, *array.shape)), axis, 0, 0, tiled=True
    )


def gathered_copies(array, axis, dim):
    return in_order(from_everyone(array, axis), dim)


def by_axis(array, axes):
    return functools.reduce(lax.psum, axes, array)


def rotate(block, positions):
    half_dim = block.shape[-1] // 2
    inverse = jnp.power(THETA, -jnp.arange(half_dim, dtype=jnp.float32) * 2.0 / block.shape[-1])
    angles = positions[:, None, None] * inverse
    cosine_val, sine_val = (jnp.cos(angles), jnp.sin(angles))
    lower_half, upper_half = (block[..., :half_dim], block[..., half_dim:])
    return jnp.concatenate(
        [
            lower_half * cosine_val - upper_half * sine_val,
            upper_half * cosine_val + lower_half * sine_val,
        ],
        axis=-1,
    )


def block_terms(rot_queries, rot_keys, value_heads, rates):
    count = rates.shape[0]
    decay_sum = jnp.cumsum(rates, axis=0)
    by_head = decay_sum.T
    causal = (jnp.arange(count)[:, None] >= jnp.arange(count)[None, :])[None]
    spread = by_head[:, :, None] - by_head[:, None, :]
    weight = jnp.where(causal, jnp.exp(jnp.where(causal, spread, 0.0)), 0.0)
    scores = jnp.einsum("ihd,jhd->hij", rot_queries, rot_keys, preferred_element_type=jnp.float32)
    weighted = (scores * weight).astype(jnp.bfloat16)
    within = jnp.einsum("hij,jhv->ihv", weighted, value_heads, preferred_element_type=jnp.float32)
    block_end = decay_sum[-1]
    carried = (
        rot_keys.astype(jnp.float32) * jnp.exp(block_end[None, :] - decay_sum)[:, :, None]
    ).astype(jnp.bfloat16)
    update = jnp.einsum("jhd,jhv->hdv", carried, value_heads, preferred_element_type=jnp.float32)
    return (within, decay_sum, jnp.exp(block_end), update)


def final_result(rot_queries, decay_sum, within, state_in, gate_part, gain_part):
    cross_part = (
        jnp.einsum(
            "ihd,hdv->ihv",
            rot_queries.astype(jnp.float32),
            state_in,
            precision=lax.Precision.HIGHEST,
        )
        * jnp.exp(decay_sum)[:, :, None]
    )
    retained = within + cross_part
    scaled = retained * lax.rsqrt(jnp.mean(retained * retained, axis=-1, keepdims=True) + EPS)
    count, head_count, value_size = retained.shape
    gated = jax.nn.silu(gate_part.astype(jnp.float32)).reshape(count, head_count, value_size)
    return (
        (scaled * gain_part.reshape(head_count, value_size) * gated)
        .reshape(count, -1)
        .astype(jnp.bfloat16)
    )


def prepare(queries, keys_in, value_part, positions, head_count):
    row_count = queries.shape[0]
    key_size = queries.shape[1] // head_count
    rot_queries = rotate(
        queries.astype(jnp.float32).reshape(row_count, head_count, key_size), positions
    ).astype(jnp.bfloat16)
    rot_keys = (
        rotate(keys_in.astype(jnp.float32).reshape(row_count, head_count, key_size), positions)
        * key_size ** (-0.5)
    ).astype(jnp.bfloat16)
    value_heads = value_part.reshape(row_count, head_count, value_part.shape[1] // head_count)
    return (rot_queries, rot_keys, value_heads)


def per_device(
    residual,
    query_small,
    key_narrow_group,
    query_large,
    key_large,
    values,
    gates,
    log_decay,
    head_gain,
    out_weight,
    norm_gain,
    routes,
    route_weight,
    expert_gate,
    expert_up,
    expert_down,
):
    row_count = residual.shape[0]
    head_count = log_decay.shape[2]
    positions = (lax.axis_index(SP) * row_count + jnp.arange(row_count, dtype=jnp.int32)).astype(
        jnp.float32
    )
    query_a, key_a, value_a = prepare(
        query_small, key_narrow_group, values[:, 0], positions, head_count
    )
    query_b, key_b, value_b = prepare(query_large, key_large, values[:, 1], positions, head_count)
    within_a, decay_sum_a, fall_a, update_a = block_terms(query_a, key_a, value_a, log_decay[:, 0])
    within_b, decay_sum_b, fall_b, update_b = block_terms(query_b, key_b, value_b, log_decay[:, 1])

    def combine(before_part, after_part):
        return (
            before_part[0] * after_part[0],
            after_part[0][:, None, None] * before_part[1] + after_part[1],
            before_part[2] * after_part[2],
            after_part[2][:, None, None] * before_part[3] + after_part[3],
        )

    identity = (
        jnp.ones_like(fall_a),
        jnp.zeros_like(update_a),
        jnp.ones_like(fall_b),
        jnp.zeros_like(update_b),
    )
    entering = entering_2((fall_a, update_a, fall_b, update_b), SP, combine, identity)
    output_a = final_result(query_a, decay_sum_a, within_a, entering[1], gates[:, 0], head_gain[0])
    output_b = final_result(query_b, decay_sum_b, within_b, entering[3], gates[:, 1], head_gain[1])
    stacked = jnp.stack([output_a, output_b], axis=1)
    gathered = gathered_copies(stacked, TP, 2)
    mixed = jnp.einsum(
        "tgk,gkd->td",
        gathered,
        lax.all_gather(out_weight, SP, axis=1, tiled=True),
        preferred_element_type=jnp.float32,
    ).astype(jnp.bfloat16)
    stream = residual.astype(jnp.float32) + mixed.astype(jnp.float32)
    square_sum = by_axis(jnp.sum(stream * stream, axis=1), TP)
    normed = (stream * lax.rsqrt(square_sum / D + EPS)[:, None] * norm_gain[None, :]).astype(
        jnp.bfloat16
    )
    experts = lax.axis_size(SP)
    capacity = 4 * row_count // experts
    one_hot = (routes[:, :, None] == jnp.arange(experts, dtype=jnp.int32)[None, None, :]).astype(
        jnp.int32
    )
    one_hot = one_hot.reshape(2 * row_count, experts)
    before = jnp.cumsum(one_hot, axis=0) - one_hot
    slot_index = jnp.sum(before * one_hot, axis=1).reshape(row_count, 2)
    target = routes * capacity + slot_index
    slot_ids = jnp.arange(experts * capacity, dtype=jnp.int32)
    choose = target[:, :, None] == slot_ids[None, None, :]
    select = jnp.sum(choose.astype(jnp.int32), axis=1).astype(jnp.bfloat16).T
    w_gate, w_up, w_down = (expert_gate[0], expert_up[0], expert_down[0])
    outgoing = jnp.dot(select, normed, preferred_element_type=jnp.float32).astype(jnp.bfloat16)
    outgoing = outgoing.reshape(experts, capacity, normed.shape[1])
    arrived = lax.all_to_all(outgoing, SP, split_axis=0, concat_axis=0, tiled=True)
    expert_arrived = lax.all_gather(arrived, TP, axis=2, tiled=True)
    gate_part = jnp.einsum(
        "sck,kf->scf", expert_arrived, w_gate, preferred_element_type=jnp.float32
    )
    up_part = jnp.einsum("sck,kf->scf", expert_arrived, w_up, preferred_element_type=jnp.float32)
    hidden = (jax.nn.silu(gate_part) * up_part).astype(jnp.bfloat16)
    expert_out = jnp.einsum(
        "scf,fd->scd", gathered_copies(hidden, TP, 2), w_down, preferred_element_type=jnp.float32
    ).astype(jnp.bfloat16)
    returned = lax.all_to_all(expert_out, SP, split_axis=0, concat_axis=0, tiled=True).reshape(
        experts * capacity, -1
    )
    first_pick = jnp.dot(
        choose[:, 0].astype(jnp.bfloat16), returned, preferred_element_type=jnp.float32
    )
    second_pick = jnp.dot(
        choose[:, 1].astype(jnp.bfloat16), returned, preferred_element_type=jnp.float32
    )
    routed = route_weight[:, 0:1] * first_pick + route_weight[:, 1:2] * second_pick
    return (stream + routed).astype(jnp.bfloat16)


def solution(mesh):
    torus = Mesh(mesh.devices.reshape(16, 2, 4, 4), ("sp_0", "sp_1", "tp_0", "tp_1"))
    placed = (
        P(SP, TP),
        P(SP, TP),
        P(SP, TP),
        P(SP, TP),
        P(SP, TP),
        P(SP, None, TP),
        P(SP, None, TP),
        P(SP, None, TP),
        P(None, TP),
        P(None, SP, TP),
        P(TP),
        P(SP, None),
        P(SP, None),
        P(SP, None, TP),
        P(SP, None, TP),
        P(SP, None, TP),
    )
    return jax.shard_map(
        per_device, mesh=torus, in_specs=placed, out_specs=P(SP, TP), check_vma=False
    )
```

profile of v0, /device:TPU:1, one launch (start us, length us, event | category | flops | bytes accessed | tf_op | source)
XLA Modules:
  0.0 372.4 jit_solution(16960491022823976062)
XLA Ops:
  6.6 0.8 slice_bitcast_fusion.9
  7.6 0.5 slice.522
  8.4 0.2 reduce_window_sum.34
  8.5 0.6 slice.523
  9.3 1.0 fusion.295
  11.7 0.9 bitcast_convert_fusion
  12.6 0.7 fusion.301
  13.2 0.8 bitcast_convert_fusion.2
  14.0 0.6 fusion.300
  14.7 0.3 fusion.287
  15.0 0.3 fusion.291
  15.3 0.3 fusion.102
  15.6 0.3 fusion.200
  15.9 8.6 %all-gather.2 = f32[2,386,128]{2,1,0:T(8,128)S(1)} all-gather(f32[1,386,128]{2,1,0:T(8,128)S(1)} %maximum_bitcast_fusion), channel_id=2, replica_groups=mesh['sp_0'=16,'sp_1'=2,'tp_0'=4,'tp_1'=4] {'sp_1'}, dimensions={0}, use_global_device_ids=true | all-gather | bytes 592896 | tf_op jit(solution)/shard_map/all_gather | solution.py:29
  24.5 0.6 fusion.298
  25.1 0.5 fusion.299
  29.2 0.7 fusion.260
  29.9 0.6 fusion.261
  30.5 0.7 maximum_bitcast_fusion.1
  31.3 0.7 all-gather.8.cloned.1.call-update
  33.6 0.3 convolution_bitcast_fusion.2
  34.0 63.0 %all-gather.12.cloned.1.call-done = f32[16,386,128]{2,1,0:T(8,128)} async-done(((f32[1,386,128]{2,1,0:T(8,128)}), f32[16,386,128]{2,1,0:T(8,128)}) %all-gather.12.cloned.1.call-update) | async-done | bytes 3162128 | tf_op jit(solution)/shard_map/all_gather | solution.py:29
  97.0 0.9 fusion.292
  97.9 0.7 fusion.296
  99.1 0.7 fusion.297
  100.4 11.6 %fusion.16 = f32[1,128,128]{2,1,0:T(8,128)S(1)} fusion(f32[16,386,128]{2,1,0:T(8,128)} %all-gather.12.cloned.1.call-done, f32[2,386,128]{2,1,0:T(8,128)S(1)} %all-gather.2, f32[128]{0:T(128)S(1)} %get-tuple-element.71, f32[]{:T(128)} %bitcast.63, f32[]{:T(128)} %bitcast.62, f32[]{:T(128)} %bitcast.61, f32[]{:T(128)} %bitcast.60, f32[]{:T(128)} %bitcast.59, ...), kind=kOutput, calls=%fused_computation.25 | convolution fusion | flops 26132480 | bytes 1322000 | tf_op jit(solution)/shard_map/ihd,hdv->ihv/dot_general | solution.py:109
  111.9 0.4 multiply_reduce_fusion.2
  112.3 12.2 %multiply_reduce_fusion.1 = (f32[128]{0:T(128)S(1)}, f32[1,128,128]{2,1,0:T(8,128)S(1)}) fusion(f32[1,128,128]{2,1,0:T(8,128)S(1)} %convolution_bitcast_fusion.2, f32[128]{0:T(128)S(1)} %get-tuple-element.73, bf16[128,128]{1,0:T(8,128)(2,1)S(1)} %get-tuple-element.67, bf16[128,128]{1,0:T(8,128)(2,1)S(1)} %get-tuple-element.68, ...), kind=kOutput, calls=%fused_computation.180 | convolution fusion | flops 52297600 | bytes 2567696 | tf_op jit(solution)/shard_map/ihd,hdv->ihv/dot_general | solution.py:109
  124.9 1.2 broadcast_in_dim.18
  126.1 6.7 %all-to-all-start = ((bf16[16,128,2,128]{3,1,2,0:T(8,128)(2,1)}), bf16[16,128,2,128]{3,1,2,0:T(8,128)(2,1)S(1)}, u32[]{:S(2)}, u32[]{:S(2)}) async-start(bf16[16,128,2,128]{3,1,2,0:T(8,128)(2,1)} %broadcast_in_dim.18), calls=%async_computation | async-start | bytes 2097152 | tf_op jit(solution)/shard_map/all_to_all | solution.py:61
  133.3 0.6 reduce-window.6
  133.9 0.2 slice_reduce_fusion
  134.5 42.4 %all-gather.8.cloned.1.call-done = bf16[2,2048,256]{2,1,0:T(8,128)(2,1)} async-done(((bf16[2,64,256]{2,1,0:T(8,128)(2,1)}), bf16[2,2048,256]{2,1,0:T(8,128)(2,1)}) %all-gather.8.cloned.1.call-update) | async-done | bytes 2097168 | tf_op jit(solution)/shard_map/all_gather | solution.py:194
  177.0 2.2 multiply_reduce_fusion
  179.1 8.3 %psum.14 = f32[128]{0:T(128)S(1)} all-reduce(f32[128]{0:T(128)S(1)} %get-tuple-element.79), channel_id=1, replica_groups=mesh['sp_0'=16,'sp_1'=2,'tp_0'=4,'tp_1'=4] {'tp_0'}, use_global_device_ids=true, to_apply=%region_9.10 | all-reduce | flops 128 | bytes 1024 | tf_op jit(solution)/shard_map/psum | solution.py:71
  187.4 8.4 %psum.15 = f32[128]{0:T(128)S(1)} all-reduce(f32[128]{0:T(128)S(1)} %psum.14), channel_id=1, replica_groups=mesh['sp_0'=16,'sp_1'=2,'tp_0'=4,'tp_1'=4] {'tp_1'}, use_global_device_ids=true, to_apply=%region_10.11 | all-reduce | flops 128 | bytes 1024 | tf_op jit(solution)/shard_map/psum | solution.py:71
  195.9 0.3 convolution_convert_fusion
  196.2 34.8 %all_to_all.20 = bf16[32,16,256]{2,1,0:T(8,128)(2,1)} all-to-all(bf16[32,16,256]{2,1,0:T(8,128)(2,1)S(1)} %bitcast.244), channel_id=1, replica_groups=mesh['sp_0'=16,'sp_1'=2,'tp_0'=4,'tp_1'=4] {'sp_0','sp_1'}, dimensions={0} | all-to-all | bytes 524288 | tf_op jit(solution)/shard_map/all_to_all | solution.py:217
  231.0 57.7 %all-gather.10.cloned.1.call-done = bf16[32,16,4096]{2,1,0:T(8,128)(2,1)} async-done(((bf16[32,16,256]{2,1,0:T(8,128)(2,1)}), bf16[32,16,4096]{2,1,0:T(8,128)(2,1)}) %all-gather.10.cloned.1.call-update) | async-done | bytes 4194320 | tf_op jit(solution)/shard_map/all_gather | solution.py:218
  288.7 3.6 fusion.23
  292.3 1.3 fusion.6
  293.6 0.4 broadcast_in_dim.19
  294.0 31.7 %all_to_all.21 = bf16[16,32,16,128]{3,2,1,0:T(8,128)(2,1)S(1)} all-to-all(bf16[16,32,16,128]{3,2,1,0:T(8,128)(2,1)S(1)} %broadcast_in_dim.19), channel_id=1, replica_groups=mesh['sp_0'=16,'sp_1'=2,'tp_0'=4,'tp_1'=4] {'tp_0','tp_1'}, dimensions={0} | all-to-all | bytes 4194304 | tf_op jit(solution)/shard_map/all_to_all | solution.py:61
  325.7 1.4 fusion.3
  327.1 15.5 %all-to-all-start.3 = ((bf16[32,16,256]{2,1,0:T(8,128)(2,1)}), bf16[32,16,256]{2,1,0:T(8,128)(2,1)S(1)}, u32[]{:S(2)}, u32[]{:S(2)}) async-start(bf16[32,16,256]{2,1,0:T(8,128)(2,1)} %fusion.3), calls=%async_computation.3 | async-start | bytes 524288 | tf_op jit(solution)/shard_map/all_to_all | solution.py:227
  342.7 22.1 %all-to-all-done.3 = bf16[32,16,256]{2,1,0:T(8,128)(2,1)S(1)} async-done(((bf16[32,16,256]{2,1,0:T(8,128)(2,1)}), bf16[32,16,256]{2,1,0:T(8,128)(2,1)S(1)}, u32[]{:S(2)}, u32[]{:S(2)}) %all-to-all-start.3) | async-done | bytes 262176 | tf_op jit(solution)/shard_map/all_to_all | solution.py:227
  364.8 0.2 convolution_multiply_fusion.2
  365.0 0.8 fusion.9
  (61 shorter events, 2.5 us)
Async XLA Ops:
  6.5 319.1 %copy-start = (bf16[1,2048,256]{2,1,0:T(8,128)(2,1)S(1)}, bf16[1,2048,256]{2,1,0:T(8,128)(2,1)}, u32[]{:S(2)}) copy-start(bf16[1,2048,256]{2,1,0:T(8,128)(2,1)} %param.31) | copy-start | bytes 3145732
  6.5 26.7 %copy-start.3 = (bf16[128,2,128]{2,1,0:T(2,128)(2,1)S(1)}, bf16[128,2,128]{2,1,0:T(2,128)(2,1)}, u32[]{:S(2)}) copy-start(bf16[128,2,128]{2,1,0:T(2,128)(2,1)} %param.22) | copy-start | bytes 196612
  6.5 27.4 %copy-start.6 = (f32[2,128]{1,0:T(2,128)S(1)}, f32[2,128]{1,0:T(2,128)}, u32[]{:S(2)}) copy-start(f32[2,128]{1,0:T(2,128)} %param.24) | copy-start | bytes 3076
  6.5 90.4 %all-gather.12.cloned.1.call-start = ((), (), s32[]{:S(2)}) async-start(), calls=%async_computation.6 | async-start | bytes 3411968 | tf_op jit(solution)/shard_map/all_gather | solution.py:29
  31.3 145.7 %all-gather.8.cloned.1.call-start = ((), (), s32[]{:S(2)}) async-start(), calls=%async_computation.4 | async-start | bytes 2162688 | tf_op jit(solution)/shard_map/all_gather | solution.py:194
  112.3 20.5 %copy-start.4 = (s32[128,2]{0,1:T(2,128)S(1)}, s32[128,2]{0,1:T(2,128)}, u32[]{:S(2)}) copy-start(s32[128,2]{0,1:T(2,128)} %param.27) | copy-start | bytes 3076
  126.1 69.8 %copy-start.5 = (f32[256]{0:T(256)S(1)}, f32[256]{0:T(256)}, u32[]{:S(2)}) copy-start(f32[256]{0:T(256)} %param.26) | copy-start | bytes 3076
  126.1 50.8 %all-to-all-start = ((bf16[16,128,2,128]{3,1,2,0:T(8,128)(2,1)}), bf16[16,128,2,128]{3,1,2,0:T(8,128)(2,1)S(1)}, u32[]{:S(2)}, u32[]{:S(2)}) async-start(bf16[16,128,2,128]{3,1,2,0:T(8,128)(2,1)} %broadcast_in_dim.18), calls=%async_computation | async-start | bytes 2097152 | tf_op jit(solution)/shard_map/all_to_all | solution.py:61
  132.8 155.9 %copy-start.2 = (bf16[1,4096,128]{2,1,0:T(8,128)(2,1)S(1)}, bf16[1,4096,128]{2,1,0:T(8,128)(2,1)}, u32[]{:S(2)}) copy-start(bf16[1,4096,128]{2,1,0:T(8,128)(2,1)} %param.29) | copy-start | bytes 3145732
  132.8 155.9 %all-gather.10.cloned.1.call-start = ((), (), s32[]{:S(2)}) async-start(), calls=%async_computation.5 | async-start | bytes 4456448 | tf_op jit(solution)/shard_map/all_gather | solution.py:218
  196.2 96.1 %copy-start.8 = (bf16[1,4096,128]{2,1,0:T(8,128)(2,1)S(1)}, bf16[1,4096,128]{2,1,0:T(8,128)(2,1)}, u32[]{:S(2)}) copy-start(bf16[1,4096,128]{2,1,0:T(8,128)(2,1)} %param.30) | copy-start | bytes 3145732
  288.7 3.6 copy-start.1
  325.7 16.9 %copy-start.7 = (f32[128,2]{0,1:T(2,128)S(1)}, f32[128,2]{0,1:T(2,128)}, u32[]{:S(2)}) copy-start(f32[128,2]{0,1:T(2,128)} %param.28) | copy-start | bytes 3076
  327.1 37.7 %all-to-all-start.3 = ((bf16[32,16,256]{2,1,0:T(8,128)(2,1)}), bf16[32,16,256]{2,1,0:T(8,128)(2,1)S(1)}, u32[]{:S(2)}, u32[]{:S(2)}) async-start(bf16[32,16,256]{2,1,0:T(8,128)(2,1)} %fusion.3), calls=%async_computation.3 | async-start | bytes 524288 | tf_op jit(solution)/shard_map/all_to_all | solution.py:227
Sparse Core Ops, SparseCore 0:
  31.4 65.5 all-gather.11
  99.1 77.7 all-gather.7
  231.1 57.5 all-gather.9
where the time goes:
time: 374 us; the launch traced here: 372 us
  waiting for transfers between devices  186 us (50%)
  blocking collectives  91.8 us (25%)
  matrix products  34.7 us (9%)
  starting transfers between devices  22.2 us (6%)
  between operations  20.9 us (6%)
  local copies, waits for them, and re-layouts  9.36 us (3%)
  other arithmetic  7.46 us (2%)
    all_gather x1, waiting for transfers between devices, gathered_once(): both, at, found = (lax.all_gather(jnp.concatenate(lines), axis), 0, {})  63 us
    all_gather x1, waiting for transfers between devices, per_device(): expert_arrived = lax.all_gather(arrived, TP, axis=2, tiled=True)  57.7 us
    all_gather x1, waiting for transfers between devices, per_device(): lax.all_gather(out_weight, SP, axis=1, tiled=True)  42.4 us
    all_to_all x1, blocking collectives, per_device(): lax.all_to_all(outgoing, SP, split_axis=0, concat_axis=0, tiled=True)  34.8 us
    all_to_all x1, blocking collectives, from_everyone(): lax.all_to_all(jnp.broadcast_to(array[None], (devices, *array.shape)), ax...  31.7 us
    dot_general x2, matrix products, final_result(): jnp.einsum('ihd,hdv->ihv', rot_queries.astype(jnp.float32), state_in, pre...  23.7 us
    all_to_all x1, waiting for transfers between devices, per_device(): lax.all_to_all(expert_out, SP, split_axis=0, concat_axis=0, tiled=True)  22.1 us
    psum x2, blocking collectives, by_axis(): return functools.reduce(lax.psum, axes, array)  16.8 us
  transfers between devices with their start and end apart: 5, of which 4 were waited for; matrix products, arithmetic and copies ran while one was open for 8% of the time, Pallas kernels for 0%

commit v1 on v0

--- a/solution.py
+++ b/solution.py
@@ -215,7 +215,9 @@
     outgoing = jnp.dot(select, normed, preferred_element_type=jnp.float32).astype(jnp.bfloat16)
     outgoing = outgoing.reshape(experts, capacity, normed.shape[1])
     arrived = lax.all_to_all(outgoing, SP, split_axis=0, concat_axis=0, tiled=True)
-    expert_arrived = lax.all_gather(arrived, TP, axis=2, tiled=True)
+    expert_arrived = jnp.concatenate(
+        lax.all_to_all(jnp.stack([arrived] * lax.axis_size(TP)), TP, 0, 0), axis=2
+    )
     gate_part = jnp.einsum(
         "sck,kf->scf", expert_arrived, w_gate, preferred_element_type=jnp.float32
     )

time: 374 us -> 358 us (0.957)
  waiting for transfers between devices: 186 us -> 128 us
  blocking collectives: 91.8 us -> 143 us
  starting transfers between devices: 22.2 us -> 13.9 us
    all_gather x1 -> x0, waiting for transfers between devices: 57.7 us -> none  [per_device(): expert_arrived = lax.all_gather(arrived, TP, axis=2, tiled=True)]
    all_to_all x0 -> x1, blocking collectives: none -> 52.7 us  [per_device(): lax.all_to_all(jnp.stack([arrived] * lax.axis_size(TP)), TP, 0, 0)]
    all_to_all x1, starting transfers between devices: 15.5 us -> 7.24 us  [per_device(): lax.all_to_all(expert_out, SP, split_axis=0, concat_axis=0, tiled=True)]
  transfers between devices with their start and end apart: 5 -> 4, of which waited for: 4 -> 3; matrix products, arithmetic and copies ran while one was open for 8% -> 9% of each run, Pallas kernels for 0% -> 0%
where the time goes in v1:
time: 358 us; the launch traced here: 357 us
  blocking collectives  143 us (40%)
  waiting for transfers between devices  128 us (36%)
  matrix products  32.3 us (9%)
  between operations  21.5 us (6%)
  starting transfers between devices  13.9 us (4%)
  local copies, waits for them, and re-layouts  10.9 us (3%)
  other arithmetic  7.34 us (2%)
    all_gather x1, waiting for transfers between devices, gathered_once(): both, at, found = (lax.all_gather(jnp.concatenate(lines), axis), 0, {})  62.9 us
    all_to_all x1, blocking collectives, per_device(): lax.all_to_all(jnp.stack([arrived] * lax.axis_size(TP)), TP, 0, 0)  52.7 us
    all_gather x1, waiting for transfers between devices, per_device(): lax.all_gather(out_weight, SP, axis=1, tiled=True)  42.4 us
    all_to_all x1, blocking collectives, per_device(): lax.all_to_all(outgoing, SP, split_axis=0, concat_axis=0, tiled=True)  34.3 us
    all_to_all x1, blocking collectives, from_everyone(): lax.all_to_all(jnp.broadcast_to(array[None], (devices, *array.shape)), ax...  30.3 us
    dot_general x2, matrix products, final_result(): jnp.einsum('ihd,hdv->ihv', rot_queries.astype(jnp.float32), state_in, pre...  23.7 us
    all_to_all x1, waiting for transfers between devices, per_device(): lax.all_to_all(expert_out, SP, split_axis=0, concat_axis=0, tiled=True)  22.1 us
    psum x2, blocking collectives, by_axis(): return functools.reduce(lax.psum, axes, array)  16.7 us
  transfers between devices with their start and end apart: 4, of which 3 were waited for; matrix products, arithmetic and copies ran while one was open for 9% of the time, Pallas kernels for 0%

profile of v1, /device:TPU:1, one launch (start us, length us, event | category | flops | bytes accessed | tf_op | source)
XLA Modules:
  0.0 356.8 jit_solution(840058625906911837)
XLA Ops:
  6.6 0.8 slice_bitcast_fusion.9
  7.6 0.5 slice.522
  8.5 0.5 slice.523
  9.2 1.0 fusion.295
  11.5 0.9 bitcast_convert_fusion
  12.4 0.7 fusion.301
  13.1 0.8 bitcast_convert_fusion.2
  13.9 0.6 fusion.300
  14.4 0.3 fusion.287
  14.8 0.3 fusion.291
  15.1 0.3 fusion.102
  15.4 0.3 fusion.200
  15.7 8.6 %all-gather.2 = f32[2,386,128]{2,1,0:T(8,128)S(1)} all-gather(f32[1,386,128]{2,1,0:T(8,128)S(1)} %maximum_bitcast_fusion), channel_id=2, replica_groups=mesh['sp_0'=16,'sp_1'=2,'tp_0'=4,'tp_1'=4] {'sp_1'}, dimensions={0}, use_global_device_ids=true | all-gather | bytes 592896 | tf_op jit(solution)/shard_map/all_gather | solution.py:29
  24.3 0.6 fusion.298
  24.9 0.5 fusion.299
  29.2 0.7 fusion.260
  29.9 0.6 fusion.261
  30.5 0.7 maximum_bitcast_fusion.1
  31.3 0.7 all-gather.7.cloned.1.call-update
  33.7 0.3 convolution_bitcast_fusion.2
  34.0 62.9 %all-gather.9.cloned.1.call-done = f32[16,386,128]{2,1,0:T(8,128)} async-done(((f32[1,386,128]{2,1,0:T(8,128)}), f32[16,386,128]{2,1,0:T(8,128)}) %all-gather.9.cloned.1.call-update) | async-done | bytes 3162128 | tf_op jit(solution)/shard_map/all_gather | solution.py:29
  96.9 0.9 fusion.292
  97.8 0.7 fusion.296
  99.1 0.7 fusion.297
  100.4 11.5 %fusion.16 = f32[1,128,128]{2,1,0:T(8,128)S(1)} fusion(f32[16,386,128]{2,1,0:T(8,128)} %all-gather.9.cloned.1.call-done, f32[2,386,128]{2,1,0:T(8,128)S(1)} %all-gather.2, f32[128]{0:T(128)S(1)} %get-tuple-element.71, f32[]{:T(128)} %bitcast.63, f32[]{:T(128)} %bitcast.62, f32[]{:T(128)} %bitcast.61, f32[]{:T(128)} %bitcast.60, f32[]{:T(128)} %bitcast.59, ...), kind=kOutput, calls=%fused_computation.25 | convolution fusion | flops 26132480 | bytes 1322000 | tf_op jit(solution)/shard_map/ihd,hdv->ihv/dot_general | solution.py:109
  111.9 0.4 multiply_reduce_fusion.2
  112.4 12.2 %multiply_reduce_fusion.1 = (f32[128]{0:T(128)S(1)}, f32[1,128,128]{2,1,0:T(8,128)S(1)}) fusion(f32[1,128,128]{2,1,0:T(8,128)S(1)} %convolution_bitcast_fusion.2, f32[128]{0:T(128)S(1)} %get-tuple-element.73, bf16[128,128]{1,0:T(8,128)(2,1)S(1)} %get-tuple-element.67, bf16[128,128]{1,0:T(8,128)(2,1)S(1)} %get-tuple-element.68, ...), kind=kOutput, calls=%fused_computation.180 | convolution fusion | flops 52297600 | bytes 2567696 | tf_op jit(solution)/shard_map/ihd,hdv->ihv/dot_general | solution.py:109
  124.9 1.2 broadcast_in_dim.18
  126.1 6.7 %all-to-all-start = ((bf16[16,128,2,128]{3,1,2,0:T(8,128)(2,1)}), bf16[16,128,2,128]{3,1,2,0:T(8,128)(2,1)S(1)}, u32[]{:S(2)}, u32[]{:S(2)}) async-start(bf16[16,128,2,128]{3,1,2,0:T(8,128)(2,1)} %broadcast_in_dim.18), calls=%async_computation | async-start | bytes 2097152 | tf_op jit(solution)/shard_map/all_to_all | solution.py:61
  133.2 0.6 reduce-window.6
  134.5 42.4 %all-gather.7.cloned.1.call-done = bf16[2,2048,256]{2,1,0:T(8,128)(2,1)} async-done(((bf16[2,64,256]{2,1,0:T(8,128)(2,1)}), bf16[2,2048,256]{2,1,0:T(8,128)(2,1)}) %all-gather.7.cloned.1.call-update) | async-done | bytes 2097168 | tf_op jit(solution)/shard_map/all_gather | solution.py:194
  176.9 2.1 multiply_reduce_fusion
  179.1 8.3 %psum.14 = f32[128]{0:T(128)S(1)} all-reduce(f32[128]{0:T(128)S(1)} %get-tuple-element.79), channel_id=1, replica_groups=mesh['sp_0'=16,'sp_1'=2,'tp_0'=4,'tp_1'=4] {'tp_0'}, use_global_device_ids=true, to_apply=%region_9.10 | all-reduce | flops 128 | bytes 1024 | tf_op jit(solution)/shard_map/psum | solution.py:71
  187.3 8.5 %psum.15 = f32[128]{0:T(128)S(1)} all-reduce(f32[128]{0:T(128)S(1)} %psum.14), channel_id=1, replica_groups=mesh['sp_0'=16,'sp_1'=2,'tp_0'=4,'tp_1'=4] {'tp_1'}, use_global_device_ids=true, to_apply=%region_10.11 | all-reduce | flops 128 | bytes 1024 | tf_op jit(solution)/shard_map/psum | solution.py:71
  195.8 0.3 convolution_convert_fusion
  196.1 34.3 %all_to_all.25 = bf16[32,16,256]{2,1,0:T(8,128)(2,1)S(1)} all-to-all(bf16[32,16,256]{2,1,0:T(8,128)(2,1)S(1)} %bitcast.250), channel_id=1, replica_groups=mesh['sp_0'=16,'sp_1'=2,'tp_0'=4,'tp_1'=4] {'sp_0','sp_1'}, dimensions={0} | all-to-all | bytes 524288 | tf_op jit(solution)/shard_map/all_to_all | solution.py:217
  230.4 0.4 stack.5
  230.8 52.7 %all_to_all.26 = bf16[16,32,16,256]{3,2,1,0:T(8,128)(2,1)S(1)} all-to-all(bf16[16,32,16,256]{3,2,1,0:T(8,128)(2,1)S(1)} %stack.5), channel_id=1, replica_groups=mesh['sp_0'=16,'sp_1'=2,'tp_0'=4,'tp_1'=4] {'tp_0','tp_1'}, dimensions={0} | all-to-all | bytes 8388608 | tf_op jit(solution)/shard_map/all_to_all | solution.py:219
  283.5 0.5 copy.77
  284.1 0.7 copy-done.1
  284.7 1.2 fusion.23
  286.0 1.3 fusion.6
  287.3 0.4 broadcast_in_dim.19
  287.7 30.3 %all_to_all.27 = bf16[16,32,16,128]{3,2,1,0:T(8,128)(2,1)S(1)} all-to-all(bf16[16,32,16,128]{3,2,1,0:T(8,128)(2,1)S(1)} %broadcast_in_dim.19), channel_id=1, replica_groups=mesh['sp_0'=16,'sp_1'=2,'tp_0'=4,'tp_1'=4] {'tp_0','tp_1'}, dimensions={0} | all-to-all | bytes 4194304 | tf_op jit(solution)/shard_map/all_to_all | solution.py:61
  318.0 1.4 fusion.3
  319.4 7.2 %all-to-all-start.4 = ((bf16[32,16,256]{2,1,0:T(8,128)(2,1)}), bf16[32,16,256]{2,1,0:T(8,128)(2,1)S(1)}, u32[]{:S(2)}, u32[]{:S(2)}) async-start(bf16[32,16,256]{2,1,0:T(8,128)(2,1)} %fusion.3), calls=%async_computation.4 | async-start | bytes 524288 | tf_op jit(solution)/shard_map/all_to_all | solution.py:229
  326.8 22.1 %all-to-all-done.4 = bf16[32,16,256]{2,1,0:T(8,128)(2,1)S(1)} async-done(((bf16[32,16,256]{2,1,0:T(8,128)(2,1)}), bf16[32,16,256]{2,1,0:T(8,128)(2,1)S(1)}, u32[]{:S(2)}, u32[]{:S(2)}) %all-to-all-start.4) | async-done | bytes 262176 | tf_op jit(solution)/shard_map/all_to_all | solution.py:229
  349.1 0.8 fusion.9
  (61 shorter events, 3.0 us)
Async XLA Ops:
  6.5 311.4 %copy-start = (bf16[1,2048,256]{2,1,0:T(8,128)(2,1)S(1)}, bf16[1,2048,256]{2,1,0:T(8,128)(2,1)}, u32[]{:S(2)}) copy-start(bf16[1,2048,256]{2,1,0:T(8,128)(2,1)} %param.31) | copy-start | bytes 3145732
  6.5 26.8 %copy-start.2 = (bf16[128,2,128]{2,1,0:T(2,128)(2,1)S(1)}, bf16[128,2,128]{2,1,0:T(2,128)(2,1)}, u32[]{:S(2)}) copy-start(bf16[128,2,128]{2,1,0:T(2,128)(2,1)} %param.22) | copy-start | bytes 196612
  6.5 27.5 %copy-start.6 = (f32[2,128]{1,0:T(2,128)S(1)}, f32[2,128]{1,0:T(2,128)}, u32[]{:S(2)}) copy-start(f32[2,128]{1,0:T(2,128)} %param.24) | copy-start | bytes 3076
  6.5 90.4 %all-gather.9.cloned.1.call-start = ((), (), s32[]{:S(2)}) async-start(), calls=%async_computation.6 | async-start | bytes 3411968 | tf_op jit(solution)/shard_map/all_gather | solution.py:29
  31.2 145.7 %all-gather.7.cloned.1.call-start = ((), (), s32[]{:S(2)}) async-start(), calls=%async_computation.5 | async-start | bytes 2162688 | tf_op jit(solution)/shard_map/all_gather | solution.py:194
  112.3 20.5 %copy-start.4 = (s32[128,2]{0,1:T(2,128)S(1)}, s32[128,2]{0,1:T(2,128)}, u32[]{:S(2)}) copy-start(s32[128,2]{0,1:T(2,128)} %param.27) | copy-start | bytes 3076
  112.3 64.6 %copy-start.3 = (bf16[128,256]{1,0:T(8,128)(2,1)S(1)}, bf16[128,256]{1,0:T(8,128)(2,1)}, u32[]{:S(2)}) copy-start(bf16[128,256]{1,0:T(8,128)(2,1)} %param.16) | copy-start | bytes 196612
  126.1 69.7 %copy-start.5 = (f32[256]{0:T(256)S(1)}, f32[256]{0:T(256)}, u32[]{:S(2)}) copy-start(f32[256]{0:T(256)} %param.26) | copy-start | bytes 3076
  126.1 50.8 %all-to-all-start = ((bf16[16,128,2,128]{3,1,2,0:T(8,128)(2,1)}), bf16[16,128,2,128]{3,1,2,0:T(8,128)(2,1)S(1)}, u32[]{:S(2)}, u32[]{:S(2)}) async-start(bf16[16,128,2,128]{3,1,2,0:T(8,128)(2,1)} %broadcast_in_dim.18), calls=%async_computation | async-start | bytes 2097152 | tf_op jit(solution)/shard_map/all_to_all | solution.py:61
  283.5 1.2 copy-start.1
  284.1 1.9 copy-start.8
  318.0 8.7 %copy-start.7 = (f32[128,2]{0,1:T(2,128)S(1)}, f32[128,2]{0,1:T(2,128)}, u32[]{:S(2)}) copy-start(f32[128,2]{0,1:T(2,128)} %param.28) | copy-start | bytes 3076
  319.4 29.5 %all-to-all-start.4 = ((bf16[32,16,256]{2,1,0:T(8,128)(2,1)}), bf16[32,16,256]{2,1,0:T(8,128)(2,1)S(1)}, u32[]{:S(2)}, u32[]{:S(2)}) async-start(bf16[32,16,256]{2,1,0:T(8,128)(2,1)} %fusion.3), calls=%async_computation.4 | async-start | bytes 524288 | tf_op jit(solution)/shard_map/all_to_all | solution.py:229
Sparse Core Ops, SparseCore 0:
  31.3 65.5 all-gather.8
  99.0 77.8 all-gather.6
